TPU v7x, 32 devices: a whole 2x2x4 slice. The times are simulated.
32 devices in a mesh: ep: 16 (over z, y, x), tp: 2 (over core).
Axes of the slice: x: 2, y: 2, z: 4, core: 2. Of those that a mesh axis runs over, the one named last changes fastest.
Arguments:
- tokens: bfloat16 [1024, 2048], P('ep', 'tp'), may hold values from -6 to 6
- sequence_state_real: float32 [1024, 128, 64], P('ep', 'tp'), may hold values from -4 to 4
- sequence_state_imaginary: float32 [1024, 128, 64], P('ep', 'tp'), may hold values from -4 to 4
- mixer_norm_gain: float32 [2048], replicated, may hold values from 0.1 to 1.9
- expert_norm_gain: float32 [2048], replicated, may hold values from 0.1 to 1.9
- rate: float32 [128, 64], P('tp'), may hold values from 0.1 to 4
- freq: float32 [128, 64], P('tp'), may hold values from -3 to 3
- log_group_step: float32 [128], P('tp'), may hold values from -3 to 0
- input_map_real: float32 [128, 64, 16], P('tp'), may hold values from -1 to 1
- input_map_imaginary: float32 [128, 64, 16], P('tp'), may hold values from -1 to 1
- output_map_real: float32 [128, 16, 64], P('tp'), may hold values from -0.75 to 0.75
- output_map_imaginary: float32 [128, 16, 64], P('tp'), may hold values from -0.75 to 0.75
- skip: float32 [2048], P('tp'), may hold values from -4 to 4
- mixer_value_weight: bfloat16 [2048, 2048], P('tp'), may hold values from -0.125 to 0.125
- mixer_gate_weight: bfloat16 [2048, 2048], P('tp'), may hold values from -0.125 to 0.125
- group_router_weight: bfloat16 [2048, 4], replicated, may hold values from -0.125 to 0.125
- expert_router_weight: bfloat16 [2048, 16], replicated, may hold values from -0.125 to 0.125
- dense_blend_weight: float32 [2048], replicated, may hold values from -0.125 to 0.125
- routes: int32 [1024, 2], P('ep'), may hold values from 0 to 15, all different within a row; in each aligned block of 64 rows (0 to 63, 64 to 127, ...) at most 16 rows name the same one
- expert_gate_weight: bfloat16 [16, 2048, 1024], P('ep', None, 'tp'), may hold values from -0.125 to 0.125
- expert_up_weight: bfloat16 [16, 2048, 1024], P('ep', None, 'tp'), may hold values from -0.125 to 0.125
- expert_down_weight: bfloat16 [16, 1024, 2048], P('ep', 'tp'), may hold values from -0.1875 to 0.1875
- shared_gate_weight: bfloat16 [2048, 2048], P('tp', 'ep'), may hold values from -0.125 to 0.125
- shared_up_weight: bfloat16 [2048, 2048], P('tp', 'ep'), may hold values from -0.125 to 0.125
- shared_down_weight: bfloat16 [2048, 2048], P(None, 'tp'), may hold values from -0.125 to 0.125
Outputs:
- result: bfloat16 [1024, 2048], P('ep', 'tp')
- next_re: float32 [1024, 128, 64], P('ep', 'tp')
- next_im: float32 [1024, 128, 64], P('ep', 'tp')
Inputs may be any that keep to these rules, and one draw needn't show every extreme that they name: `routes`: each row names 2 different experts. Among the rows of one device no expert is named more than 16 times, and in every draw some expert is named exactly 16 times by some device's rows.
All inputs are finite; a program needn't handle non-finite values.
Results may differ from a plain program's by a relative error of at most 0.017.
Values may be sent and summed in bfloat16 or wider, within the bound.
A program may use at most 128 MiB of HBM per device.

v0:
```python
import jax
import jax.numpy as jnp
from jax import lax
from jax.sharding import PartitionSpec as P

NG = 4
EPS = 1e-06
PRECISION_MAX = lax.Precision.HIGHEST


def state_factors(rate, freq, log_group_step, input_map_real, input_map_imaginary):
    step_size = jnp.exp(log_group_step)[:, None]
    magnitude = jnp.exp(-rate * step_size)
    abar_re = magnitude * jnp.cos(freq * step_size)
    abar_im = magnitude * jnp.sin(freq * step_size)
    denom = rate * rate + freq * freq
    shift_re = abar_re - 1.0
    fac_re = (abar_im * freq - shift_re * rate) / denom
    fac_im = -(abar_im * rate + shift_re * freq) / denom
    bbar_re = fac_re[:, :, None] * input_map_real - fac_im[:, :, None] * input_map_imaginary
    bbar_im = fac_re[:, :, None] * input_map_imaginary + fac_im[:, :, None] * input_map_real
    return (abar_re, abar_im, bbar_re, bbar_im)


def state_step(
    normed,
    sequence_state_real,
    sequence_state_imaginary,
    factors,
    output_map_real,
    output_map_imaginary,
    skip,
):
    abar_re, abar_im, bbar_re, bbar_im = factors
    groups = abar_re.shape[0]
    inputs = normed.astype(jnp.float32)
    grouped = inputs.reshape(inputs.shape[0], groups, -1)
    drive_re = jnp.einsum("tgc,gpc->tgp", grouped, bbar_re, precision=PRECISION_MAX)
    drive_im = jnp.einsum("tgc,gpc->tgp", grouped, bbar_im, precision=PRECISION_MAX)
    fresh_real = abar_re * sequence_state_real - abar_im * sequence_state_imaginary + drive_re
    fresh_imaginary = abar_re * sequence_state_imaginary + abar_im * sequence_state_real + drive_im
    state_readout = jnp.einsum("dor,zdr->zdo", output_map_real, fresh_real, precision=PRECISION_MAX)
    state_readout = state_readout - jnp.einsum(
        "dor,zdr->zdo", output_map_imaginary, fresh_imaginary, precision=PRECISION_MAX
    )
    mixed = state_readout.reshape(inputs.shape) + skip * inputs
    return (mixed, fresh_real, fresh_imaginary)


def pair_product(left, first_map, second_map):
    first = jnp.dot(left, first_map, preferred_element_type=jnp.float32)
    second = jnp.dot(left, second_map, preferred_element_type=jnp.float32)
    return jnp.concatenate([first, second], axis=1)


def shards(
    tokens,
    sequence_state_real,
    sequence_state_imaginary,
    mixer_norm_gain,
    expert_norm_gain,
    rate,
    freq,
    log_group_step,
    input_map_real,
    input_map_imaginary,
    output_map_real,
    output_map_imaginary,
    skip,
    mixer_value_weight,
    mixer_gate_weight,
    group_router_weight,
    expert_router_weight,
    dense_blend_weight,
    routes,
    expert_gate_weight,
    expert_up_weight,
    expert_down_weight,
    shared_gate_weight,
    shared_up_weight,
    shared_down_weight,
):
    seq_rows, half_width = tokens.shape
    width = 2 * half_width
    column_start = lax.axis_index("tp") * half_width

    def own_rows(values):
        return lax.dynamic_slice_in_dim(values, column_start, half_width, 0)

    float_tokens = tokens.astype(jnp.float32)
    square_sum = lax.psum(jnp.sum(float_tokens * float_tokens, axis=1), "tp")
    first_scale = lax.rsqrt(square_sum / width + EPS)[:, None]
    normed = (float_tokens * first_scale * own_rows(mixer_norm_gain)).astype(jnp.bfloat16)
    factors = state_factors(rate, freq, log_group_step, input_map_real, input_map_imaginary)
    mixed, next_re, next_im = state_step(
        normed,
        sequence_state_real,
        sequence_state_imaginary,
        factors,
        output_map_real,
        output_map_imaginary,
        skip,
    )
    activated = jax.nn.gelu(mixed).astype(jnp.bfloat16)
    value_part = jnp.dot(activated, mixer_value_weight, preferred_element_type=jnp.float32)
    gate_part = jnp.dot(activated, mixer_gate_weight, preferred_element_type=jnp.float32)
    stacked = jnp.stack([value_part, gate_part], axis=1)
    mix_sum = lax.psum_scatter(
        stacked.astype(jnp.bfloat16), "tp", scatter_dimension=2, tiled=True
    ).astype(jnp.float32)
    mix_half = (mix_sum[:, 0] * jax.nn.sigmoid(mix_sum[:, 1])).astype(jnp.bfloat16)
    hidden = (float_tokens + mix_half.astype(jnp.float32)).astype(jnp.bfloat16)
    hidden_f32 = hidden.astype(jnp.float32)
    scaled = hidden_f32 * own_rows(expert_norm_gain)
    router_map = jnp.concatenate(
        [own_rows(group_router_weight), own_rows(expert_router_weight)], axis=1
    ).astype(jnp.float32)
    blend_map = own_rows(dense_blend_weight)
    hidden_squares = jnp.sum(hidden_f32 * hidden_f32, axis=1)
    total_squares = lax.psum(hidden_squares, "tp")
    inverse = lax.rsqrt(total_squares / width + EPS)[:, None]
    normal_rows = scaled * inverse
    raw_part = jnp.dot(normal_rows, router_map, precision=PRECISION_MAX)
    blend_part = jnp.dot(normal_rows, blend_map, precision=PRECISION_MAX)
    logits, blend_logit = lax.psum((raw_part, blend_part), "tp")
    hnorm = (scaled * inverse).astype(jnp.bfloat16)
    experts = expert_router_weight.shape[1]
    top_count = routes.shape[1]
    per_group = experts // NG
    group_prob = jax.nn.softmax(logits[:, :NG], axis=-1)
    expert_logits = logits[:, NG:]
    expert_hits = routes[:, :, None] == jnp.arange(experts, dtype=jnp.int32)[None, None, :]
    chosen = jnp.sum(jnp.where(expert_hits, expert_logits[:, None, :], 0.0), axis=2)
    group_hits = (routes // per_group)[:, :, None] == jnp.arange(NG, dtype=jnp.int32)[None, None, :]
    group_sel = jnp.sum(jnp.where(group_hits, group_prob[:, None, :], 0.0), axis=2)
    weights = jax.nn.softmax(chosen, axis=1) * group_sel
    full_rows = lax.all_gather(hnorm, "tp", axis=1, tiled=True)
    capacity = max(2, 2 * seq_rows * top_count // experts)
    flat_routes = routes.reshape(-1)
    matches = (flat_routes[:, None] == jnp.arange(experts, dtype=jnp.int32)[None, :]).astype(
        jnp.int32
    )
    slot_rank = jnp.sum(jnp.cumsum(matches, axis=0) * matches, axis=1) - 1
    slot_target = flat_routes * capacity + slot_rank
    dispatch = slot_target[None, :] == jnp.arange(experts * capacity, dtype=jnp.int32)[:, None]
    dispatch_rows = jnp.sum(
        dispatch.reshape(experts * capacity, seq_rows, top_count).astype(jnp.float32), axis=2
    )
    outgoing = jnp.dot(
        dispatch_rows.astype(jnp.bfloat16), full_rows, preferred_element_type=jnp.float32
    )
    outgoing = outgoing.astype(jnp.bfloat16).reshape(experts, capacity, width)
    received = lax.all_to_all(outgoing, "ep", split_axis=0, concat_axis=0, tiled=True)
    sources = received.shape[0]
    items = received.shape[1]
    token_rows = received.reshape(sources * items, width)
    gate_e = jnp.dot(token_rows, expert_gate_weight[0], preferred_element_type=jnp.float32)
    expert_up_rows = jnp.dot(token_rows, expert_up_weight[0], preferred_element_type=jnp.float32)
    inner = (jax.nn.silu(gate_e) * expert_up_rows).astype(jnp.bfloat16)
    part_out = jnp.dot(inner, expert_down_weight[0], preferred_element_type=jnp.float32)
    total = lax.psum_scatter(part_out.astype(jnp.bfloat16), "tp", scatter_dimension=1, tiled=True)
    finished = total.reshape(sources, items, half_width)
    returned = lax.all_to_all(finished, "ep", split_axis=0, concat_axis=0, tiled=True)
    returned_flat = returned.reshape(experts * capacity, half_width)
    picked = returned_flat[slot_target].reshape(seq_rows, top_count, half_width).astype(jnp.float32)
    routed = jnp.sum(weights[:, :, None] * picked, axis=1)
    partial_dense = pair_product(
        lax.all_gather(hnorm, "ep", axis=0, tiled=True), shared_gate_weight, shared_up_weight
    )
    dense_sum = lax.psum(partial_dense.astype(jnp.bfloat16), "tp").astype(jnp.float32)
    dense_cols = shared_gate_weight.shape[1]
    inner_cols = (jax.nn.silu(dense_sum[:, :dense_cols]) * dense_sum[:, dense_cols:]).astype(
        jnp.bfloat16
    )
    dense_inner = lax.all_to_all(inner_cols, "ep", split_axis=0, concat_axis=1, tiled=True)
    dense_out = jnp.dot(dense_inner, shared_down_weight, preferred_element_type=jnp.float32)
    result = hidden_f32 + routed + jax.nn.sigmoid(blend_logit)[:, None] * dense_out
    return (result.astype(jnp.bfloat16), next_re, next_im)


def solution(mesh):
    placed = (
        P("ep", "tp"),
        P("ep", "tp", None),
        P("ep", "tp", None),
        P(),
        P(),
        P("tp", None),
        P("tp", None),
        P("tp"),
        P("tp", None, None),
        P("tp", None, None),
        P("tp", None, None),
        P("tp", None, None),
        P("tp"),
        P("tp", None),
        P("tp", None),
        P(),
        P(),
        P(),
        P("ep", None),
        P("ep", None, "tp"),
        P("ep", None, "tp"),
        P("ep", "tp", None),
        P("tp", "ep"),
        P("tp", "ep"),
        P(None, "tp"),
    )
    return jax.shard_map(
        shards,
        mesh=mesh,
        in_specs=placed,
        out_specs=(P("ep", "tp"), P("ep", "tp", None), P("ep", "tp", None)),
        check_vma=False,
    )
```

profile of v0, /device:TPU:0, one launch (start us, length us, event | category | flops | bytes accessed | tf_op | source)
XLA Modules:
  0.0 187.7 jit_solution(3510667995029894204)
XLA Ops:
  7.2 3.5 %copy.64 = f32[64,64,64]{0,2,1:T(8,128)} copy(f32[64,64,64]{2,1,0:T(8,128)} %param.27) | data formatting | bytes 2097152 | tf_op args[2]
  10.7 3.4 %copy.63 = f32[64,64,64]{0,2,1:T(8,128)} copy(f32[64,64,64]{2,1,0:T(8,128)} %param.26) | data formatting | bytes 2097152 | tf_op args[1]
  14.3 2.6 %psum.35 = f32[64]{0:T(128)S(1)} all-reduce(f32[64]{0:T(128)S(1)} %fusion.29), channel_id=1, replica_groups=mesh['ep'=16,'tp'=2] {'tp'}, use_global_device_ids=true, to_apply=%region_1.0 | all-reduce | flops 64 | bytes 512 | tf_op jit(solution)/shard_map/psum | solution.py:91
  19.8 4.9 %bitcast_add_fusion.1 = f32[64,64,64]{0,2,1:T(8,128)S(1)} fusion(f32[64,64,64]{0,2,1:T(8,128)} %copy.64, f32[64,64,64]{0,2,1:T(8,128)} %copy.63, bf16[64,64,16]{0,2,1:T(8,128)(2,1)S(1)} %bitcast.75, f32[64,64]{1,0:T(8,128)S(1)} %get-tuple-element.17, f32[64,64]{1,0:T(8,128)S(1)} %get-tuple-element.18, f32[64,64,16]{1,2,0:T(8,128)S(1)} %copy-done.7, ...), kind=kOutput, calls=%fused_computation.13 | convolution fusion | flops 51576832 | bytes 3866624 | tf_op jit(solution)/shard_map/tgc,gpc->tgp/dot_general | solution.py:38
  24.8 3.2 %bitcast_add_fusion = f32[64,64,64]{0,2,1:T(8,128)S(1)} fusion(f32[64,64,64]{0,2,1:T(8,128)S(1)} %copy-done.4, f32[64,64,64]{0,2,1:T(8,128)S(1)} %copy-done.3, bf16[64,64,16]{0,2,1:T(8,128)(2,1)S(1)} %bitcast.76, f32[64,64]{1,0:T(8,128)S(1)} %get-tuple-element.17, f32[64,64]{1,0:T(8,128)S(1)} %get-tuple-element.18, f32[64,64,16]{1,2,0:T(8,128)S(1)} %copy-done.8, ...), kind=kOutput, calls=%fused_computation.12 | convolution fusion | flops 51576832 | bytes 3866624 | tf_op jit(solution)/shard_map/tgc,gpc->tgp/dot_general | solution.py:39
  30.0 1.9 %convolution_subtract_fusion = f32[64,64,16]{1,2,0:T(8,128)S(1)} fusion(f32[64,64,16]{1,2,0:T(8,128)S(1)} %fusion.77, f32[64,64,64]{0,2,1:T(8,128)S(1)} %bitcast_add_fusion, f32[64,16,64]{2,1,0:T(8,128)S(1)} %copy-done.10), kind=kOutput, calls=%fused_computation.15 | convolution fusion | flops 50397184 | bytes 1835008 | tf_op jit(solution)/shard_map/dor,zdr->zdo/dot_general | solution.py:43
  32.1 3.3 %fusion.1 = bf16[64,1,2048]{2,0,1:T(8,128)(2,1)S(1)} fusion(bf16[1024,2048]{1,0:T(8,128)(2,1)} %param.39, f32[64,1024]{1,0:T(8,128)S(1)} %copy.70, f32[1024]{0:T(1024)S(1)} %copy-done.14, f32[1024]{0:T(1024)S(1)} %dynamic_slice.15, f32[64]{0:T(128)S(1)} %add_rsqrt_fusion.1, bf16[64,1024]{1,0:T(8,128)(2,1)S(1)} %copy-done.6), kind=kOutput, calls=%fused_computation.6 | convolution fusion | flops 269615104 | bytes 4858112 | tf_op jit(solution)/shard_map/dot_general | solution.py:106
  37.8 10.3 %reduce-scatter.3.cloned.1.call-done = bf16[64,2,1024]{2,0,1:T(8,128)(2,1)} async-done(((bf16[64,2,2048]{2,0,1:T(8,128)(2,1)}), bf16[64,2,1024]{2,0,1:T(8,128)(2,1)}) %reduce-scatter.3.cloned.1.call-update) | async-done | bytes 262160 | tf_op jit(solution)/shard_map/reduce_scatter | solution.py:108
  49.3 2.5 %psum.36 = f32[64]{0:T(128)S(1)} all-reduce(f32[64]{0:T(128)S(1)} %get-tuple-element.14), channel_id=1, replica_groups=mesh['ep'=16,'tp'=2] {'tp'}, use_global_device_ids=true, to_apply=%region_4.0 | all-reduce | flops 64 | bytes 512 | tf_op jit(solution)/shard_map/psum | solution.py:120
  53.4 2.3 %all_gather.6 = bf16[64,2048]{1,0:T(8,128)(2,1)S(1)} all-gather(bf16[64,1024]{1,0:T(8,128)(2,1)} %fusion.43), channel_id=1, replica_groups=mesh['ep'=16,'tp'=2] {'tp'}, dimensions={1}, use_global_device_ids=true | all-gather | bytes 393216 | tf_op jit(solution)/shard_map/all_gather | solution.py:137
  56.2 41.0 %all_to_all.29 = bf16[16,16,2048]{2,1,0:T(8,128)(2,1)S(1)} all-to-all(bf16[16,16,2048]{2,1,0:T(8,128)(2,1)S(1)} %bitcast.74), channel_id=1, replica_groups=mesh['ep'=16,'tp'=2] {'ep'}, dimensions={0} | all-to-all | bytes 2097152 | tf_op jit(solution)/shard_map/all_to_all | solution.py:153
  98.9 4.2 %convolution_convert_fusion = bf16[256,2048]{1,0:T(8,128)(2,1)} fusion(bf16[1,512,2048]{2,1,0:T(8,128)(2,1)S(1)} %copy-done, bf16[256,2048]{1,0:T(8,128)(2,1)} %bitcast.79, bf16[1,2048,512]{2,1,0:T(8,128)(2,1)} %param.45, f32[256,512]{1,0:T(8,128)S(1)} %fusion.5), kind=kOutput, calls=%fused_computation.1 | convolution fusion | flops 1075052544 | bytes 6815744 | tf_op jit(solution)/shard_map/dot_general | solution.py:160
  103.1 3.8 %copy.77 = f32[64,64,64]{2,1,0:T(8,128)} copy(f32[64,64,64]{0,2,1:T(8,128)} %copy-done.2) | data formatting | bytes 2097152
  106.9 3.8 %copy.78 = f32[64,64,64]{2,1,0:T(8,128)} copy(f32[64,64,64]{0,2,1:T(8,128)} %copy-done.1) | data formatting | bytes 2097152
  111.7 3.3 %all-reduce = (f32[64,20]{0,1:T(8,128)S(1)}, f32[64]{0:T(128)S(1)}) all-reduce(f32[64,20]{0,1:T(8,128)S(1)} %fusion.44, f32[64]{0:T(128)S(1)} %convolution_bitcast_fusion), channel_id=1, replica_groups=mesh['ep'=16,'tp'=2] {'tp'}, use_global_device_ids=true, to_apply=%region_5.0 | all-reduce | flops 1344 | bytes 10752 | tf_op jit(solution)/shard_map/psum | solution.py:125
  115.1 3.4 %all-gather.2.cloned.1.call-done = bf16[1024,1024]{1,0:T(8,128)(2,1)} async-done(((bf16[64,1024]{1,0:T(8,128)(2,1)}), bf16[1024,1024]{1,0:T(8,128)(2,1)}) %all-gather.2.cloned.1.call-update) | async-done | bytes 2097168 | tf_op jit(solution)/shard_map/all_gather | solution.py:168
  118.5 2.4 %convolution_convert_fusion.4 = bf16[1024,128]{0,1:T(8,128)(2,1)S(1)} fusion(bf16[1024,1024]{1,0:T(8,128)(2,1)} %all-gather.2.cloned.1.call-done, bf16[1024,128]{1,0:T(8,128)(2,1)S(1)} %copy-done.12), kind=kOutput, calls=%fused_computation.17 | convolution fusion | flops 268566528 | bytes 2621440 | tf_op jit(solution)/shard_map/dot_general | solution.py:52
  120.9 7.1 %reduce-scatter.5.cloned.1.call-done = bf16[256,1024]{1,0:T(8,128)(2,1)} async-done(((bf16[256,2048]{1,0:T(8,128)(2,1)}), bf16[256,1024]{1,0:T(8,128)(2,1)}) %reduce-scatter.5.cloned.1.call-update) | async-done | bytes 524304 | tf_op jit(solution)/shard_map/reduce_scatter | solution.py:161
  128.0 6.8 %all-to-all-start.1 = ((bf16[16,16,1024]{2,1,0:T(8,128)(2,1)}), bf16[16,16,1024]{2,1,0:T(8,128)(2,1)S(1)}, u32[]{:S(2)}, u32[]{:S(2)}) async-start(bf16[16,16,1024]{2,1,0:T(8,128)(2,1)} %bitcast.80), calls=%async_computation.3 | async-start | bytes 1048576 | tf_op jit(solution)/shard_map/all_to_all | solution.py:163
  134.9 2.4 %convolution_convert_fusion.5 = bf16[1024,128]{0,1:T(8,128)(2,1)S(1)} fusion(bf16[1024,1024]{1,0:T(8,128)(2,1)} %all-gather.2.cloned.1.call-done, bf16[1024,128]{1,0:T(8,128)(2,1)S(1)} %copy-done.13), kind=kOutput, calls=%fused_computation.18 | convolution fusion | flops 268566528 | bytes 2621440 | tf_op jit(solution)/shard_map/dot_general | solution.py:51
  138.2 20.0 %all-reduce.3.cloned.1.call-done = bf16[1024,256]{0,1:T(8,128)(2,1)} async-done(((bf16[1024,256]{0,1:T(8,128)(2,1)}), bf16[1024,256]{0,1:T(8,128)(2,1)}) %all-reduce.3.cloned.1.call-update) | async-done | bytes 524304 | tf_op jit(solution)/shard_map/psum | solution.py:170
  160.3 6.8 %all-to-all-start.2 = ((bf16[16,64,128]{2,1,0:T(8,128)(2,1)}), bf16[16,64,128]{2,1,0:T(8,128)(2,1)S(1)}, u32[]{:S(2)}, u32[]{:S(2)}) async-start(bf16[16,64,128]{2,1,0:T(8,128)(2,1)} %bitcast.19), calls=%async_computation.4 | async-start | bytes 524288 | tf_op jit(solution)/shard_map/all_to_all | solution.py:175
  169.2 8.2 %all-to-all-done.2 = bf16[16,64,128]{2,1,0:T(8,128)(2,1)S(1)} async-done(((bf16[16,64,128]{2,1,0:T(8,128)(2,1)}), bf16[16,64,128]{2,1,0:T(8,128)(2,1)S(1)}, u32[]{:S(2)}, u32[]{:S(2)}) %all-to-all-start.2) | async-done | bytes 262176 | tf_op jit(solution)/shard_map/all_to_all | solution.py:175
  177.5 3.7 %fusion.14 = bf16[64,1024]{1,0:T(8,128)(2,1)} fusion(bf16[2048,1024]{1,0:T(8,128)(2,1)} %param.49, f32[64,1024]{1,0:T(8,128)S(1)} %multiply_reduce_fusion, bf16[64,1024]{1,0:T(8,128)(2,1)S(1)} %get-tuple-element.15, f32[64]{0:T(128)S(1)} %add_divide_fusion, bf16[16,64,128]{2,1,0:T(8,128)(2,1)S(1)} %all-to-all-done.2), kind=kOutput, calls=%fused_computation.21 | convolution fusion | flops 268763136 | bytes 4980992 | tf_op jit(solution)/shard_map/dot_general | solution.py:176
  (109 shorter events, 18.4 us)
Async XLA Ops:
  7.2 91.7 %copy-start = (bf16[1,512,2048]{2,1,0:T(8,128)(2,1)S(1)}, bf16[1,512,2048]{2,1,0:T(8,128)(2,1)}, u32[]{:S(2)}) copy-start(bf16[1,512,2048]{2,1,0:T(8,128)(2,1)} %param.46) | copy-start | bytes 6291460
  7.2 40.9 %reduce-scatter.3.cloned.1.call-start = ((), (), s32[]{:S(2)}) async-start(), calls=%async_computation.5 | async-start | bytes 786432 | tf_op jit(solution)/shard_map/reduce_scatter | solution.py:108
  10.7 3.4 %copy-start.6 = (bf16[64,1024]{1,0:T(8,128)(2,1)S(1)}, bf16[64,1024]{1,0:T(8,128)(2,1)}, u32[]{:S(2)}) copy-start(bf16[64,1024]{1,0:T(8,128)(2,1)} %param.25) | copy-start | bytes 393220
  10.7 6.2 %copy-start.18 = (f32[2048]{0:T(1024)S(1)}, f32[2048]{0:T(1024)}, u32[]{:S(2)}) copy-start(f32[2048]{0:T(1024)} %param.28) | copy-start | bytes 24580
  10.7 8.0 %copy-start.21 = (f32[64]{0:T(128)S(1)}, f32[64]{0:T(128)}, u32[]{:S(2)}) copy-start(f32[64]{0:T(128)} %param.32) | copy-start | bytes 772
  10.7 9.1 %copy-start.7 = (f32[64,64,16]{1,2,0:T(8,128)S(1)}, f32[64,64,16]{1,2,0:T(8,128)}, u32[]{:S(2)}) copy-start(f32[64,64,16]{1,2,0:T(8,128)} %param.34) | copy-start | bytes 786436
  10.7 9.1 %copy-start.8 = (f32[64,64,16]{1,2,0:T(8,128)S(1)}, f32[64,64,16]{1,2,0:T(8,128)}, u32[]{:S(2)}) copy-start(f32[64,64,16]{1,2,0:T(8,128)} %param.33) | copy-start | bytes 786436
  19.8 5.0 %copy-start.3 = (f32[64,64,64]{0,2,1:T(8,128)S(1)}, f32[64,64,64]{0,2,1:T(8,128)}, u32[]{:S(2)}) copy-start(f32[64,64,64]{0,2,1:T(8,128)} %copy.64) | copy-start | bytes 3145732
  19.8 5.0 %copy-start.4 = (f32[64,64,64]{0,2,1:T(8,128)S(1)}, f32[64,64,64]{0,2,1:T(8,128)}, u32[]{:S(2)}) copy-start(f32[64,64,64]{0,2,1:T(8,128)} %copy.63) | copy-start | bytes 3145732
  24.8 3.3 %copy-start.2 = (f32[64,64,64]{0,2,1:T(8,128)}, f32[64,64,64]{0,2,1:T(8,128)S(1)}, u32[]{:S(2)}) copy-start(f32[64,64,64]{0,2,1:T(8,128)S(1)} %bitcast_add_fusion.1) | copy-start | bytes 3145732
  24.8 3.3 %copy-start.11 = (f32[64,16,64]{2,1,0:T(8,128)S(1)}, f32[64,16,64]{2,1,0:T(8,128)}, u32[]{:S(2)}) copy-start(f32[64,16,64]{2,1,0:T(8,128)} %param.35) | copy-start | bytes 786436
  28.0 3.9 %copy-start.1 = (f32[64,64,64]{0,2,1:T(8,128)}, f32[64,64,64]{0,2,1:T(8,128)S(1)}, u32[]{:S(2)}) copy-start(f32[64,64,64]{0,2,1:T(8,128)S(1)} %bitcast_add_fusion) | copy-start | bytes 3145732
  32.1 3.5 %copy-start.5 = (bf16[1024,2048]{1,0:T(8,128)(2,1)S(1)}, bf16[1024,2048]{1,0:T(8,128)(2,1)}, u32[]{:S(2)}) copy-start(bf16[1024,2048]{1,0:T(8,128)(2,1)} %param.38) | copy-start | bytes 12582916
  37.4 81.1 %all-gather.2.cloned.1.call-start = ((), (), s32[]{:S(2)}) async-start(), calls=%async_computation.7 | async-start | bytes 2228224 | tf_op jit(solution)/shard_map/all_gather | solution.py:168
  52.5 75.5 %reduce-scatter.5.cloned.1.call-start = ((), (), s32[]{:S(2)}) async-start(), calls=%async_computation.6 | async-start | bytes 1572864 | tf_op jit(solution)/shard_map/reduce_scatter | solution.py:161
  53.3 44.9 %copy-start.20 = (bf16[1,2048,512]{2,1,0:T(8,128)(2,1)S(1)}, bf16[1,2048,512]{2,1,0:T(8,128)(2,1)}, u32[]{:S(2)}) copy-start(bf16[1,2048,512]{2,1,0:T(8,128)(2,1)} %param.44) | copy-start | bytes 6291460
  106.9 4.0 %copy-start.17 = (bf16[2048,4]{0,1:T(4,128)(2,1)S(1)}, bf16[2048,4]{0,1:T(4,128)(2,1)}, u32[]{:S(2)}) copy-start(bf16[2048,4]{0,1:T(4,128)(2,1)} %param.40) | copy-start | bytes 49156
  106.9 4.0 %copy-start.15 = (bf16[2048,16]{0,1:T(8,128)(2,1)S(1)}, bf16[2048,16]{0,1:T(8,128)(2,1)}, u32[]{:S(2)}) copy-start(bf16[2048,16]{0,1:T(8,128)(2,1)} %param.41) | copy-start | bytes 196612
  106.9 4.1 %dynamic-slice-start = ((f32[2048]{0:T(1024)}, s32[]{:T(128)}), f32[1024]{0:T(1024)S(1)}, s32[]{:S(2)}) async-start(f32[2048]{0:T(1024)} %param.42, s32[]{:T(128)} %select_n.30), calls=%async_computation.9 | async-start | bytes 8704 | tf_op jit(solution)/shard_map/dynamic_slice | solution.py:88
  106.9 11.6 %copy-start.12 = (bf16[1024,128]{1,0:T(8,128)(2,1)S(1)}, bf16[1024,128]{1,0:T(8,128)(2,1)}, u32[]{:S(2)}) copy-start(bf16[1024,128]{1,0:T(8,128)(2,1)} %param.48) | copy-start | bytes 786436
  111.0 23.9 %copy-start.13 = (bf16[1024,128]{1,0:T(8,128)(2,1)S(1)}, bf16[1024,128]{1,0:T(8,128)(2,1)}, u32[]{:S(2)}) copy-start(bf16[1024,128]{1,0:T(8,128)(2,1)} %param.47) | copy-start | bytes 786436
  128.0 32.3 %all-to-all-start.1 = ((bf16[16,16,1024]{2,1,0:T(8,128)(2,1)}), bf16[16,16,1024]{2,1,0:T(8,128)(2,1)S(1)}, u32[]{:S(2)}, u32[]{:S(2)}) async-start(bf16[16,16,1024]{2,1,0:T(8,128)(2,1)} %bitcast.80), calls=%async_computation.3 | async-start | bytes 1048576 | tf_op jit(solution)/shard_map/all_to_all | solution.py:163
  134.8 23.4 %all-reduce.3.cloned.1.call-start = ((), (), s32[]{:S(2)}) async-start(), calls=%async_computation.8 | async-start | bytes 1048576 | tf_op jit(solution)/shard_map/psum | solution.py:170
  160.3 17.1 %all-to-all-start.2 = ((bf16[16,64,128]{2,1,0:T(8,128)(2,1)}), bf16[16,64,128]{2,1,0:T(8,128)(2,1)S(1)}, u32[]{:S(2)}, u32[]{:S(2)}) async-start(bf16[16,64,128]{2,1,0:T(8,128)(2,1)} %bitcast.19), calls=%async_computation.4 | async-start | bytes 524288 | tf_op jit(solution)/shard_map/all_to_all | solution.py:175
  (5 other events, 8.9 us)
Sparse Core Ops, SparseCore 0:
  37.6 10.4 reduce-scatter.2
  52.6 65.8 all-gather.1
  120.8 7.2 reduce-scatter.4
  138.3 19.8 all-reduce.2
where the time goes:
time: 188 us
  blocking collectives  51.7 us (28%)
  waiting for transfers between devices  49.1 us (26%)
  matrix products  30.9 us (16%)
  local copies, waits for them, and re-layouts  19.7 us (10%)
  between operations  14.3 us (8%)
  starting transfers between devices  13.8 us (7%)
  other arithmetic  8.23 us (4%)
    all_to_all x1, blocking collectives, shards(): lax.all_to_all(outgoing, 'ep', split_axis=0, concat_axis=0, tiled=True)  41 us
    psum x1, waiting for transfers between devices, shards(): lax.psum(partial_dense.astype(jnp.bfloat16), 'tp').astype(jnp.float32)  20 us
    unnamed x49, local copies, waits for them, and re-layouts  15.8 us
    reduce_scatter x1, waiting for transfers between devices, shards(): lax.psum_scatter(stacked.astype(jnp.bfloat16), 'tp', scatter_dimension=2,...  10.3 us
    all_to_all x1, waiting for transfers between devices, shards(): lax.all_to_all(inner_cols, 'ep', split_axis=0, concat_axis=1, tiled=True)  8.24 us
    reduce_scatter x1, waiting for transfers between devices, shards(): lax.psum_scatter(part_out.astype(jnp.bfloat16), 'tp', scatter_dimension=1...  7.08 us
    all_to_all x1, starting transfers between devices, shards(): lax.all_to_all(inner_cols, 'ep', split_axis=0, concat_axis=1, tiled=True)  6.83 us
    all_to_all x1, starting transfers between devices, shards(): lax.all_to_all(finished, 'ep', split_axis=0, concat_axis=0, tiled=True)  6.79 us
  transfers between devices with their start and end apart: 6, of which 5 were waited for; matrix products, arithmetic and copies ran while one was open for 13% of the time, Pallas kernels for 0%

commit v1 on v0

--- a/solution.py
+++ b/solution.py
@@ -167,7 +167,9 @@
     partial_dense = pair_product(
         lax.all_gather(hnorm, "ep", axis=0, tiled=True), shared_gate_weight, shared_up_weight
     )
-    dense_sum = lax.psum(partial_dense.astype(jnp.bfloat16), "tp").astype(jnp.float32)
+    dense_sum = jnp.sum(lax.all_gather(partial_dense.astype(jnp.bfloat16), "tp"), axis=0).astype(
+        jnp.float32
+    )
     dense_cols = shared_gate_weight.shape[1]
     inner_cols = (jax.nn.silu(dense_sum[:, :dense_cols]) * dense_sum[:, dense_cols:]).astype(
         jnp.bfloat16

time: 188 us -> 174 us (0.926)
  waiting for transfers between devices: 49.1 us -> 35.9 us
  starting transfers between devices: 13.8 us -> 10.9 us
    psum x1 -> x0, waiting for transfers between devices: 20 us -> none  [shards(): lax.psum(partial_dense.astype(jnp.bfloat16), 'tp').astype(jnp.float32)]
    reduce_scatter x1, waiting for transfers between devices: 7.08 us -> 0.87 us  [shards(): lax.psum_scatter(part_out.astype(jnp.bfloat16), 'tp', scatter_dimension=1...]
    all_to_all x1, waiting for transfers between devices: 0.01 us -> 5.93 us  [shards(): lax.all_to_all(finished, 'ep', split_axis=0, concat_axis=0, tiled=True)]
    all_gather x0 -> x1, waiting for transfers between devices: none -> 4.68 us  [shards(): lax.all_gather(partial_dense.astype(jnp.bfloat16), 'tp')]
    all_gather x1, waiting for transfers between devices: 3.41 us -> 6.93 us  [shards(): lax.all_gather(hnorm, 'ep', axis=0, tiled=True)]
    all_to_all x1, starting transfers between devices: 6.83 us -> 3.99 us  [shards(): lax.all_to_all(inner_cols, 'ep', split_axis=0, concat_axis=1, tiled=True)]
    reduce_sum x0 -> x1, other arithmetic: none -> 2.37 us  [shards(): jnp.sum(lax.all_gather(partial_dense.astype(jnp.bfloat16), 'tp'), axis=0)]
    unnamed x49 -> x50, local copies, waits for them, and re-layouts: 15.8 us -> 16 us
  transfers between devices with their start and end apart: 6 -> 6, of which waited for: 5 -> 6; matrix products, arithmetic and copies ran while one was open for 13% -> 15% of each run, Pallas kernels for 0% -> 0%
where the time goes in v1:
time: 174 us; the launch traced here: 173 us
  blocking collectives  51.9 us (30%)
  waiting for transfers between devices  35.9 us (21%)
  matrix products  30 us (17%)
  local copies, waits for them, and re-layouts  21 us (12%)
  between operations  14.3 us (8%)
  starting transfers between devices  10.9 us (6%)
  other arithmetic  8.75 us (5%)
    all_to_all x1, blocking collectives, shards(): lax.all_to_all(outgoing, 'ep', split_axis=0, concat_axis=0, tiled=True)  41.1 us
    unnamed x50, local copies, waits for them, and re-layouts  16 us
    reduce_scatter x1, waiting for transfers between devices, shards(): lax.psum_scatter(stacked.astype(jnp.bfloat16), 'tp', scatter_dimension=2,...  10.3 us
    all_to_all x1, waiting for transfers between devices, shards(): lax.all_to_all(inner_cols, 'ep', split_axis=0, concat_axis=1, tiled=True)  7.1 us
    all_gather x1, waiting for transfers between devices, shards(): lax.all_gather(hnorm, 'ep', axis=0, tiled=True)  6.93 us
    all_to_all x1, starting transfers between devices, shards(): lax.all_to_all(finished, 'ep', split_axis=0, concat_axis=0, tiled=True)  6.79 us
    all_to_all x1, waiting for transfers between devices, shards(): lax.all_to_all(finished, 'ep', split_axis=0, concat_axis=0, tiled=True)  5.93 us
    dot_general x1, matrix products, state_step(): jnp.einsum('tgc,gpc->tgp', grouped, bbar_re, precision=PRECISION_MAX)  4.93 us
  transfers between devices with their start and end apart: 6, of which 6 were waited for; matrix products, arithmetic and copies ran while one was open for 15% of the time, Pallas kernels for 0%

profile of v1, /device:TPU:0, one launch (start us, length us, event | category | flops | bytes accessed | tf_op | source)
XLA Modules:
  0.0 172.8 jit_solution(12865813921069355237)
XLA Ops:
  7.2 3.5 %copy.99 = f32[64,64,64]{0,2,1:T(8,128)} copy(f32[64,64,64]{2,1,0:T(8,128)} %param.27) | data formatting | bytes 2097152 | tf_op args[2]
  10.7 3.4 %copy.98 = f32[64,64,64]{0,2,1:T(8,128)} copy(f32[64,64,64]{2,1,0:T(8,128)} %param.26) | data formatting | bytes 2097152 | tf_op args[1]
  14.3 2.6 %psum.28 = f32[64]{0:T(128)S(1)} all-reduce(f32[64]{0:T(128)S(1)} %fusion.31), channel_id=1, replica_groups=mesh['ep'=16,'tp'=2] {'tp'}, use_global_device_ids=true, to_apply=%region_1.0 | all-reduce | flops 64 | bytes 512 | tf_op jit(solution)/shard_map/psum | solution.py:91
  19.8 4.9 %bitcast_add_fusion.1 = f32[64,64,64]{0,2,1:T(8,128)S(1)} fusion(f32[64,64,64]{0,2,1:T(8,128)} %copy.99, f32[64,64,64]{0,2,1:T(8,128)} %copy.98, bf16[64,64,16]{0,2,1:T(8,128)(2,1)S(1)} %bitcast.79, f32[64,64]{1,0:T(8,128)S(1)} %get-tuple-element.23, f32[64,64]{1,0:T(8,128)S(1)} %get-tuple-element.24, f32[64,64,16]{1,2,0:T(8,128)S(1)} %copy-done.8, ...), kind=kOutput, calls=%fused_computation.13 | convolution fusion | flops 51576832 | bytes 3866624 | tf_op jit(solution)/shard_map/tgc,gpc->tgp/dot_general | solution.py:38
  24.8 3.2 %bitcast_add_fusion = f32[64,64,64]{0,2,1:T(8,128)S(1)} fusion(f32[64,64,64]{0,2,1:T(8,128)S(1)} %copy-done.4, f32[64,64,64]{0,2,1:T(8,128)S(1)} %copy-done.3, bf16[64,64,16]{0,2,1:T(8,128)(2,1)S(1)} %bitcast.80, f32[64,64]{1,0:T(8,128)S(1)} %get-tuple-element.23, f32[64,64]{1,0:T(8,128)S(1)} %get-tuple-element.24, f32[64,64,16]{1,2,0:T(8,128)S(1)} %copy-done.9, ...), kind=kOutput, calls=%fused_computation.12 | convolution fusion | flops 51576832 | bytes 3866624 | tf_op jit(solution)/shard_map/tgc,gpc->tgp/dot_general | solution.py:39
  30.0 1.9 %convolution_subtract_fusion = f32[64,64,16]{1,2,0:T(8,128)S(1)} fusion(f32[64,64,16]{1,2,0:T(8,128)S(1)} %fusion.79, f32[64,64,64]{0,2,1:T(8,128)S(1)} %bitcast_add_fusion, f32[64,16,64]{2,1,0:T(8,128)S(1)} %copy-done.10), kind=kOutput, calls=%fused_computation.15 | convolution fusion | flops 50397184 | bytes 1835008 | tf_op jit(solution)/shard_map/dor,zdr->zdo/dot_general | solution.py:43
  32.1 3.3 %fusion.1 = bf16[64,1,2048]{2,0,1:T(8,128)(2,1)S(1)} fusion(bf16[1024,2048]{1,0:T(8,128)(2,1)} %param.39, f32[64,1024]{1,0:T(8,128)S(1)} %copy.105, f32[1024]{0:T(1024)S(1)} %copy-done.14, f32[1024]{0:T(1024)S(1)} %dynamic_slice.15, f32[64]{0:T(128)S(1)} %add_rsqrt_fusion.1, bf16[64,1024]{1,0:T(8,128)(2,1)S(1)} %copy-done.7), kind=kOutput, calls=%fused_computation.6 | convolution fusion | flops 269615104 | bytes 4858112 | tf_op jit(solution)/shard_map/dot_general | solution.py:106
  37.8 10.3 %reduce-scatter.3.cloned.1.call-done = bf16[64,2,1024]{2,0,1:T(8,128)(2,1)} async-done(((bf16[64,2,2048]{2,0,1:T(8,128)(2,1)}), bf16[64,2,1024]{2,0,1:T(8,128)(2,1)}) %reduce-scatter.3.cloned.1.call-update) | async-done | bytes 262160 | tf_op jit(solution)/shard_map/reduce_scatter | solution.py:108
  49.3 2.5 %psum.29 = f32[64]{0:T(128)S(1)} all-reduce(f32[64]{0:T(128)S(1)} %get-tuple-element.20), channel_id=1, replica_groups=mesh['ep'=16,'tp'=2] {'tp'}, use_global_device_ids=true, to_apply=%region_4.0 | all-reduce | flops 64 | bytes 512 | tf_op jit(solution)/shard_map/psum | solution.py:120
  53.4 2.3 %all_gather.10 = bf16[64,2048]{1,0:T(8,128)(2,1)S(1)} all-gather(bf16[64,1024]{1,0:T(8,128)(2,1)} %fusion.45), channel_id=1, replica_groups=mesh['ep'=16,'tp'=2] {'tp'}, dimensions={1}, use_global_device_ids=true | all-gather | bytes 393216 | tf_op jit(solution)/shard_map/all_gather | solution.py:137
  56.2 41.1 %all_to_all.29 = bf16[16,16,2048]{2,1,0:T(8,128)(2,1)S(1)} all-to-all(bf16[16,16,2048]{2,1,0:T(8,128)(2,1)S(1)} %bitcast.78), channel_id=1, replica_groups=mesh['ep'=16,'tp'=2] {'ep'}, dimensions={0} | all-to-all | bytes 2097152 | tf_op jit(solution)/shard_map/all_to_all | solution.py:153
  98.8 4.0 %convolution_convert_fusion = bf16[256,2048]{1,0:T(8,128)(2,1)} fusion(bf16[1,512,2048]{2,1,0:T(8,128)(2,1)S(1)} %copy-done, bf16[256,2048]{1,0:T(8,128)(2,1)S(1)} %bitcast.83, bf16[1,2048,512]{2,1,0:T(8,128)(2,1)} %param.45, f32[256,512]{1,0:T(8,128)} %fusion.5), kind=kOutput, calls=%fused_computation.1 | convolution fusion | flops 1075052544 | bytes 6815744 | tf_op jit(solution)/shard_map/dot_general | solution.py:160
  102.9 3.8 %copy.114 = f32[64,64,64]{2,1,0:T(8,128)} copy(f32[64,64,64]{0,2,1:T(8,128)} %copy-done.2) | data formatting | bytes 2097152
  106.6 3.8 %copy.115 = f32[64,64,64]{2,1,0:T(8,128)} copy(f32[64,64,64]{0,2,1:T(8,128)} %copy-done.1) | data formatting | bytes 2097152
  110.7 6.9 %all-gather.3.cloned.1.call-done = bf16[1024,1024]{1,0:T(8,128)(2,1)} async-done(((bf16[64,1024]{1,0:T(8,128)(2,1)}), bf16[1024,1024]{1,0:T(8,128)(2,1)}) %all-gather.3.cloned.1.call-update) | async-done | bytes 2097168 | tf_op jit(solution)/shard_map/all_gather | solution.py:168
  117.6 2.6 %fusion.14 = bf16[1,1024,128]{1,2,0:T(8,128)(2,1)S(1)} fusion(bf16[1024,1024]{1,0:T(8,128)(2,1)} %all-gather.3.cloned.1.call-done, bf16[1024,128]{1,0:T(8,128)(2,1)S(1)} %copy-done.12), kind=kOutput, calls=%fused_computation.20 | convolution fusion | flops 268566528 | bytes 2621440 | tf_op jit(solution)/shard_map/dot_general | solution.py:52
  122.9 3.3 %all-reduce = (f32[64,20]{0,1:T(8,128)S(1)}, f32[64]{0:T(128)S(1)}) all-reduce(f32[64,20]{0,1:T(8,128)S(1)} %fusion.46, f32[64]{0:T(128)S(1)} %convolution_bitcast_fusion), channel_id=1, replica_groups=mesh['ep'=16,'tp'=2] {'tp'}, use_global_device_ids=true, to_apply=%region_5.0 | all-reduce | flops 1344 | bytes 10752 | tf_op jit(solution)/shard_map/psum | solution.py:125
  127.1 6.8 %all-to-all-start.1 = ((bf16[16,16,1024]{2,1,0:T(8,128)(2,1)}), bf16[16,16,1024]{2,1,0:T(8,128)(2,1)S(1)}, u32[]{:S(2)}, u32[]{:S(2)}) async-start(bf16[16,16,1024]{2,1,0:T(8,128)(2,1)} %bitcast.84), calls=%async_computation.3 | async-start | bytes 1048576 | tf_op jit(solution)/shard_map/all_to_all | solution.py:163
  134.0 4.7 %all-gather.5.cloned.1.call-done = bf16[2,1024,256]{2,1,0:T(8,128)(2,1)} async-done(((bf16[1,1024,256]{2,1,0:T(8,128)(2,1)}), bf16[2,1024,256]{2,1,0:T(8,128)(2,1)}) %all-gather.5.cloned.1.call-update) | async-done | bytes 1048592 | tf_op jit(solution)/shard_map/all_gather | solution.py:170
  138.7 2.4 %reduce_sum.102 = bf16[1024,256]{1,0:T(8,128)(2,1)} reduce(bf16[2,1024,256]{2,1,0:T(8,128)(2,1)} %all-gather.5.cloned.1.call-done, bf16[]{:T(256)} %constant.64.clone.1), dimensions={0}, to_apply=%region_18.19 | reduce | flops 262144 | bytes 1572866 | tf_op jit(solution)/shard_map/reduce_sum | solution.py:170
  143.5 5.9 %all-to-all-done.1 = bf16[16,16,1024]{2,1,0:T(8,128)(2,1)S(1)} async-done(((bf16[16,16,1024]{2,1,0:T(8,128)(2,1)}), bf16[16,16,1024]{2,1,0:T(8,128)(2,1)S(1)}, u32[]{:S(2)}, u32[]{:S(2)}) %all-to-all-start.1) | async-done | bytes 524320 | tf_op jit(solution)/shard_map/all_to_all | solution.py:163
  149.4 4.0 %all-to-all-start.2 = ((bf16[16,64,128]{2,1,0:T(8,128)(2,1)}), bf16[16,64,128]{2,1,0:T(8,128)(2,1)S(1)}, u32[]{:S(2)}, u32[]{:S(2)}) async-start(bf16[16,64,128]{2,1,0:T(8,128)(2,1)} %bitcast.21), calls=%async_computation.4 | async-start | bytes 524288 | tf_op jit(solution)/shard_map/all_to_all | solution.py:177
  155.4 7.1 %all-to-all-done.2 = bf16[16,64,128]{2,1,0:T(8,128)(2,1)S(1)} async-done(((bf16[16,64,128]{2,1,0:T(8,128)(2,1)}), bf16[16,64,128]{2,1,0:T(8,128)(2,1)S(1)}, u32[]{:S(2)}, u32[]{:S(2)}) %all-to-all-start.2) | async-done | bytes 262176 | tf_op jit(solution)/shard_map/all_to_all | solution.py:177
  162.5 3.7 %fusion.16 = bf16[64,1024]{1,0:T(8,128)(2,1)} fusion(bf16[2048,1024]{1,0:T(8,128)(2,1)} %param.49, f32[64,1024]{1,0:T(8,128)S(1)} %multiply_reduce_fusion, bf16[64,1024]{1,0:T(8,128)(2,1)S(1)} %get-tuple-element.21, f32[64]{0:T(128)S(1)} %add_divide_fusion, bf16[16,64,128]{2,1,0:T(8,128)(2,1)S(1)} %all-to-all-done.2), kind=kOutput, calls=%fused_computation.23 | convolution fusion | flops 268763136 | bytes 4980992 | tf_op jit(solution)/shard_map/dot_general | solution.py:178
  (112 shorter events, 20.4 us)
Async XLA Ops:
  7.2 91.6 %copy-start = (bf16[1,512,2048]{2,1,0:T(8,128)(2,1)S(1)}, bf16[1,512,2048]{2,1,0:T(8,128)(2,1)}, u32[]{:S(2)}) copy-start(bf16[1,512,2048]{2,1,0:T(8,128)(2,1)} %param.46) | copy-start | bytes 6291460
  7.2 40.9 %reduce-scatter.3.cloned.1.call-start = ((), (), s32[]{:S(2)}) async-start(), calls=%async_computation.5 | async-start | bytes 786432 | tf_op jit(solution)/shard_map/reduce_scatter | solution.py:108
  10.7 3.4 %copy-start.7 = (bf16[64,1024]{1,0:T(8,128)(2,1)S(1)}, bf16[64,1024]{1,0:T(8,128)(2,1)}, u32[]{:S(2)}) copy-start(bf16[64,1024]{1,0:T(8,128)(2,1)} %param.25) | copy-start | bytes 393220
  10.7 6.2 %copy-start.18 = (f32[2048]{0:T(1024)S(1)}, f32[2048]{0:T(1024)}, u32[]{:S(2)}) copy-start(f32[2048]{0:T(1024)} %param.28) | copy-start | bytes 24580
  10.7 8.0 %copy-start.21 = (f32[64]{0:T(128)S(1)}, f32[64]{0:T(128)}, u32[]{:S(2)}) copy-start(f32[64]{0:T(128)} %param.32) | copy-start | bytes 772
  10.7 9.1 %copy-start.8 = (f32[64,64,16]{1,2,0:T(8,128)S(1)}, f32[64,64,16]{1,2,0:T(8,128)}, u32[]{:S(2)}) copy-start(f32[64,64,16]{1,2,0:T(8,128)} %param.34) | copy-start | bytes 786436
  10.7 9.1 %copy-start.9 = (f32[64,64,16]{1,2,0:T(8,128)S(1)}, f32[64,64,16]{1,2,0:T(8,128)}, u32[]{:S(2)}) copy-start(f32[64,64,16]{1,2,0:T(8,128)} %param.33) | copy-start | bytes 786436
  19.8 5.0 %copy-start.3 = (f32[64,64,64]{0,2,1:T(8,128)S(1)}, f32[64,64,64]{0,2,1:T(8,128)}, u32[]{:S(2)}) copy-start(f32[64,64,64]{0,2,1:T(8,128)} %copy.99) | copy-start | bytes 3145732
  19.8 5.0 %copy-start.4 = (f32[64,64,64]{0,2,1:T(8,128)S(1)}, f32[64,64,64]{0,2,1:T(8,128)}, u32[]{:S(2)}) copy-start(f32[64,64,64]{0,2,1:T(8,128)} %copy.98) | copy-start | bytes 3145732
  24.8 3.3 %copy-start.2 = (f32[64,64,64]{0,2,1:T(8,128)}, f32[64,64,64]{0,2,1:T(8,128)S(1)}, u32[]{:S(2)}) copy-start(f32[64,64,64]{0,2,1:T(8,128)S(1)} %bitcast_add_fusion.1) | copy-start | bytes 3145732
  24.8 3.3 %copy-start.11 = (f32[64,16,64]{2,1,0:T(8,128)S(1)}, f32[64,16,64]{2,1,0:T(8,128)}, u32[]{:S(2)}) copy-start(f32[64,16,64]{2,1,0:T(8,128)} %param.35) | copy-start | bytes 786436
  28.0 3.9 %copy-start.1 = (f32[64,64,64]{0,2,1:T(8,128)}, f32[64,64,64]{0,2,1:T(8,128)S(1)}, u32[]{:S(2)}) copy-start(f32[64,64,64]{0,2,1:T(8,128)S(1)} %bitcast_add_fusion) | copy-start | bytes 3145732
  32.1 3.5 %copy-start.6 = (bf16[1024,2048]{1,0:T(8,128)(2,1)S(1)}, bf16[1024,2048]{1,0:T(8,128)(2,1)}, u32[]{:S(2)}) copy-start(bf16[1024,2048]{1,0:T(8,128)(2,1)} %param.38) | copy-start | bytes 12582916
  37.4 80.2 %all-gather.3.cloned.1.call-start = ((), (), s32[]{:S(2)}) async-start(), calls=%async_computation.7 | async-start | bytes 2228224 | tf_op jit(solution)/shard_map/all_gather | solution.py:168
  52.5 74.6 %reduce-scatter.5.cloned.1.call-start = ((), (), s32[]{:S(2)}) async-start(), calls=%async_computation.6 | async-start | bytes 1572864 | tf_op jit(solution)/shard_map/reduce_scatter | solution.py:161
  53.3 44.0 %copy-start.20 = (bf16[1,2048,512]{2,1,0:T(8,128)(2,1)S(1)}, bf16[1,2048,512]{2,1,0:T(8,128)(2,1)}, u32[]{:S(2)}) copy-start(bf16[1,2048,512]{2,1,0:T(8,128)(2,1)} %param.44) | copy-start | bytes 6291460
  102.8 35.9 %all-gather.5.cloned.1.call-start = ((), (), s32[]{:S(2)}) async-start(), calls=%async_computation.8 | async-start | bytes 1572864 | tf_op jit(solution)/shard_map/all_gather | solution.py:170
  106.6 4.0 %copy-start.17 = (bf16[2048,4]{0,1:T(4,128)(2,1)S(1)}, bf16[2048,4]{0,1:T(4,128)(2,1)}, u32[]{:S(2)}) copy-start(bf16[2048,4]{0,1:T(4,128)(2,1)} %param.40) | copy-start | bytes 49156
  106.6 4.0 %copy-start.15 = (bf16[2048,16]{0,1:T(8,128)(2,1)S(1)}, bf16[2048,16]{0,1:T(8,128)(2,1)}, u32[]{:S(2)}) copy-start(bf16[2048,16]{0,1:T(8,128)(2,1)} %param.41) | copy-start | bytes 196612
  106.6 11.0 %copy-start.12 = (bf16[1024,128]{1,0:T(8,128)(2,1)S(1)}, bf16[1024,128]{1,0:T(8,128)(2,1)}, u32[]{:S(2)}) copy-start(bf16[1024,128]{1,0:T(8,128)(2,1)} %param.48) | copy-start | bytes 786436
  110.5 9.8 %copy-start.13 = (bf16[1024,128]{1,0:T(8,128)(2,1)S(1)}, bf16[1024,128]{1,0:T(8,128)(2,1)}, u32[]{:S(2)}) copy-start(bf16[1024,128]{1,0:T(8,128)(2,1)} %param.47) | copy-start | bytes 786436
  117.6 2.6 %copy-start.5 = (bf16[1024,1024]{1,0:T(8,128)(2,1)S(1)}, bf16[1024,1024]{1,0:T(8,128)(2,1)}, u32[]{:S(2)}) copy-start(bf16[1024,1024]{1,0:T(8,128)(2,1)} %all-gather.3.cloned.1.call-done) | copy-start | bytes 6291460
  127.1 22.3 %all-to-all-start.1 = ((bf16[16,16,1024]{2,1,0:T(8,128)(2,1)}), bf16[16,16,1024]{2,1,0:T(8,128)(2,1)S(1)}, u32[]{:S(2)}, u32[]{:S(2)}) async-start(bf16[16,16,1024]{2,1,0:T(8,128)(2,1)} %bitcast.84), calls=%async_computation.3 | async-start | bytes 1048576 | tf_op jit(solution)/shard_map/all_to_all | solution.py:163
  149.4 13.1 %all-to-all-start.2 = ((bf16[16,64,128]{2,1,0:T(8,128)(2,1)}), bf16[16,64,128]{2,1,0:T(8,128)(2,1)S(1)}, u32[]{:S(2)}, u32[]{:S(2)}) async-start(bf16[16,64,128]{2,1,0:T(8,128)(2,1)} %bitcast.21), calls=%async_computation.4 | async-start | bytes 524288 | tf_op jit(solution)/shard_map/all_to_all | solution.py:177
  (5 other events, 9.9 us)
Sparse Core Ops, SparseCore 0:
  37.6 10.4 reduce-scatter.2
  52.6 64.9 all-gather.2
  119.9 7.1 reduce-scatter.4
  128.5 10.1 all-gather.4
